TPU v7x, 512 devices: a whole 4x4x16 slice. The times are simulated.
512 devices in a mesh: sp: 64 (over z, y), tp: 8 (over x, core).
Axes of the slice: x: 4, y: 4, z: 16, core: 2. Of those that a mesh axis runs over, the one named last changes fastest.
Arguments:
- queries: bfloat16 [24576, 2048], P('sp', 'tp'), may hold values from -6 to 6
- key_heads: bfloat16 [24576, 1024], P('sp', 'tp'), may hold values from -6 to 6
- value_heads: bfloat16 [24576, 1024], P('sp', 'tp'), may hold values from -6 to 6
- sink_logit: float32 [16], P('tp'), may hold values from 3 to 7
- doc_ids: int32 [24576], replicated, may hold values from 0 to 15, never falling along the last dimension, each value on 1 to 3072 neighbouring positions
- residual: bfloat16 [24576, 2048], P('sp'), may hold values from -6 to 6
- out_proj: bfloat16 [2048, 2048], P('tp'), may hold values from -0.125 to 0.125
- gain_mix: float32 [2048], replicated, may hold values from 0.1 to 1.9
- up_proj: bfloat16 [2048, 8192], P('sp', 'tp'), may hold values from -0.125 to 0.125
- down_proj: bfloat16 [8192, 2048], P('tp', 'sp'), may hold values from -0.0625 to 0.0625
- gain_ffn_in: float32 [2048], replicated, may hold values from 0.1 to 1.9
- gain_ffn_out: float32 [2048], replicated, may hold values from 0.1 to 1.9
Outputs:
- layer_out: bfloat16 [24576, 2048], P(('sp', 'tp'))
All inputs are finite; a program needn't handle non-finite values.
Results may differ from a plain program's by a relative error of at most 0.019.
Values may be sent and summed in bfloat16 or wider, within the bound.
No kernel may reach another device: no remote copies, remote signals or barrier semaphores. Data moves between devices by JAX's collectives and lax.ppermute only.
A program may use at most 64 MiB of HBM per device.

v0:
```python
import jax
import jax.numpy as jnp
from jax import lax
from jax.sharding import PartitionSpec as P

HD = 128
WINDOW = 128


def turned_gather(arrays, axis, dims):
    turned = [jnp.moveaxis(a, dim, 0) for a, dim in zip(arrays, dims)]
    both = jnp.concatenate([t.reshape(len(t), -1) for t in turned], axis=1)
    result, at, gathered = (lax.all_gather(both, axis, axis=0, tiled=True), 0, [])
    for t, dim in zip(turned, dims):
        section = result[:, at : at + t[0].size].reshape(-1, *t.shape[1:])
        gathered.append(jnp.moveaxis(section, 0, dim))
        at += t[0].size
    return tuple(gathered)


def padded(shard, sides, width):
    for axis, dim in sides:
        devices, length = (lax.axis_size(axis), shard.shape[dim])
        up = [(i, (i + 1) % devices) for i in range(devices - 1)]
        down = [(j, i) for i, j in up]
        last = lax.slice_in_dim(shard, length - width, length, axis=dim)
        first = lax.slice_in_dim(shard, 0, width, axis=dim)
        before = lax.ppermute(last, axis, up)
        after = lax.ppermute(first, axis, down)
        shard = jnp.concatenate([before, shard, after], axis=dim)
    return shard


def split_up(shard, dim, devices):
    before, after = (shard.shape[:dim], shard.shape[dim + 1 :])
    return jnp.moveaxis(shard.reshape(*before, devices, -1, *after), dim, 0)


def summed_on_arrival(shard, axis, dim):
    pieces = split_up(shard, dim, lax.axis_size(axis))
    arrived = lax.all_to_all(pieces, axis, split_axis=0, concat_axis=0, tiled=True)
    return arrived.astype(jnp.float32).sum(axis=0)


def joined_along(pieces, dim):
    pieces = jnp.moveaxis(pieces, 0, dim)
    lengths = pieces.shape
    return pieces.reshape(*lengths[:dim], lengths[dim] * lengths[dim + 1], *lengths[dim + 2 :])


def copy_for_each(shard, axis):
    devices = lax.axis_size(axis)
    return lax.all_to_all(
        jnp.broadcast_to(shard[None], (devices, *shard.shape)), axis, 0, 0, tiled=True
    )


def collect(shard, axis, dim):
    return joined_along(copy_for_each(shard, axis), dim)


def rotate(field, places):
    half_dim = HD // 2
    inv_freq = 10000.0 ** (-jnp.arange(0, HD, 2, dtype=jnp.float32) / HD)
    angles = places[:, None, None] * inv_freq[None, None, :]
    cosine = jnp.cos(angles)
    sine = jnp.sin(angles)
    lower = field[..., :half_dim].astype(jnp.float32)
    upper = field[..., half_dim:].astype(jnp.float32)
    return jnp.concatenate(
        [lower * cosine - upper * sine, upper * cosine + lower * sine], axis=-1
    ).astype(jnp.bfloat16)


def banded(field, blocks):
    framed = field.reshape((blocks + 2, WINDOW) + field.shape[1:])
    return jnp.concatenate([framed[:-2], framed[1:-1], framed[2:]], axis=1)


def rms_scale(field, gain_vec):
    return field * lax.rsqrt(jnp.mean(field * field, axis=-1, keepdims=True) + 1e-06) * gain_vec


def body(
    queries,
    key_heads,
    value_heads,
    sink_logit,
    doc_ids,
    residual,
    out_proj,
    gain_mix,
    up_proj,
    down_proj,
    gain_ffn_in,
    gain_ffn_out,
):
    tok_count = queries.shape[0]
    blocks = tok_count // WINDOW
    share_rows = tok_count // lax.axis_size("tp")
    q_local = queries.shape[1] // HD
    kv_local = key_heads.shape[1] // HD
    group_size = q_local // kv_local
    offset = lax.axis_index("sp") * tok_count
    up_whole, down_whole = turned_gather((up_proj, down_proj), "sp", (0, 1))
    places = (offset + jnp.arange(tok_count)).astype(jnp.float32)
    rotated_q = rotate(queries.reshape(tok_count, q_local, HD), places).reshape(
        blocks, WINDOW, kv_local, group_size, HD
    )
    rotated_k = rotate(key_heads.reshape(tok_count, kv_local, HD), places).reshape(
        tok_count, kv_local * HD
    )
    rimmed = padded(jnp.stack([rotated_k, value_heads]), (("sp", 1),), WINDOW)
    key_win = banded(rimmed[0].reshape(-1, kv_local, HD), blocks)
    val_win = banded(rimmed[1].reshape(-1, kv_local, HD), blocks)
    padded_docs = jnp.pad(doc_ids, (WINDOW, WINDOW), constant_values=-1)
    key_docs = banded(lax.dynamic_slice_in_dim(padded_docs, offset, tok_count + 2 * WINDOW), blocks)
    query_docs = lax.dynamic_slice_in_dim(doc_ids, offset, tok_count).reshape(blocks, WINDOW)
    q_index = jnp.arange(WINDOW)[:, None]
    k_index = jnp.arange(3 * WINDOW)[None, :]
    in_window = jnp.abs(k_index - WINDOW - q_index) <= WINDOW
    allowed = (in_window[None] & (query_docs[:, :, None] == key_docs[:, None, :]))[:, None, None]
    scores = jnp.einsum(
        "nqkgd,nskd->nkgqs", rotated_q, key_win, preferred_element_type=jnp.float32
    ) * HD ** (-0.5)
    masked = jnp.where(allowed, scores, -1e30)
    sink_col = sink_logit.reshape(kv_local, group_size)[None, :, :, None]
    top_score = jnp.maximum(jnp.max(masked, axis=-1), sink_col)
    exp_scores = jnp.where(allowed, jnp.exp(masked - top_score[..., None]), 0.0)
    denom_sum = jnp.sum(exp_scores, axis=-1) + jnp.exp(sink_col - top_score)
    probs = (exp_scores / denom_sum[..., None]).astype(jnp.bfloat16)
    attn = (
        jnp.einsum("nkgqs,nskd->nqkgd", probs, val_win, preferred_element_type=jnp.float32)
        .astype(jnp.bfloat16)
        .reshape(tok_count, q_local * HD)
    )
    mixed = summed_on_arrival(
        jnp.dot(attn, out_proj, preferred_element_type=jnp.float32).astype(jnp.bfloat16), "tp", 0
    )
    own_resid = lax.dynamic_slice_in_dim(residual, lax.axis_index("tp") * share_rows, share_rows, 0)
    after_mix = (own_resid.astype(jnp.float32) + rms_scale(mixed, gain_mix)).astype(jnp.bfloat16)
    own_normed = rms_scale(after_mix.astype(jnp.float32), gain_ffn_in).astype(jnp.bfloat16)
    normed = collect(own_normed, "tp", 0)
    up_acts = jnp.dot(normed, up_whole, preferred_element_type=jnp.float32)
    hidden = jnp.square(jax.nn.relu(up_acts)).astype(jnp.bfloat16)
    ffn_out = summed_on_arrival(
        jnp.dot(hidden, down_whole, preferred_element_type=jnp.float32).astype(jnp.bfloat16),
        "tp",
        0,
    )
    return (after_mix.astype(jnp.float32) + rms_scale(ffn_out, gain_ffn_out)).astype(jnp.bfloat16)


def solution(mesh):
    return jax.shard_map(
        body,
        mesh=mesh,
        in_specs=(
            P("sp", "tp"),
            P("sp", "tp"),
            P("sp", "tp"),
            P("tp"),
            P(),
            P("sp", None),
            P("tp", None),
            P(),
            P("sp", "tp"),
            P("tp", "sp"),
            P(),
            P(),
        ),
        out_specs=P(("sp", "tp"), None),
        check_vma=False,
    )
```

profile of v0, /device:TPU:1, one launch (start us, length us, event | category | flops | bytes accessed | tf_op | source)
XLA Modules:
  0.0 213.6 jit_solution(9553838884716437725)
XLA Ops:
  6.5 1.6 pad_maximum_fusion
  8.2 1.8 fusion.41
  10.1 0.9 pad_maximum_fusion.11
  11.0 4.0 %collective-permute-start = (bf16[2,128,128]{2,1,0:T(8,128)(2,1)S(1)}, bf16[2,128,128]{2,1,0:T(8,128)(2,1)S(1)}, u32[]{:S(2)}, u32[]{:S(2)}) collective-permute-start(bf16[2,128,128]{2,1,0:T(8,128)(2,1)S(1)} %get-tuple-element.15), channel_id=1, source_target_pairs={{0,8},{8,16},{16,24},{24,32},{32,40},{40,48},{48,56},{56,64},{64,7... | collective-permute-start | bytes 196616 | tf_op jit(solution)/shard_map/ppermute | solution.py:28
  15.0 1.3 collective-permute-start.1
  16.3 1.1 copy.26
  17.7 0.4 multiply_cosine_fusion.1
  18.2 0.2 compare_and_fusion
  19.1 1.0 collective-permute-done.1
  20.4 0.4 fusion.53
  20.9 0.3 fusion.14
  21.3 0.4 fusion.13
  21.9 1.8 convolution_convert_fusion
  23.7 8.7 %all-to-all-start = ((bf16[8,48,2048]{2,1,0:T(8,128)(2,1)}), bf16[8,48,2048]{2,1,0:T(8,128)(2,1)S(1)}, u32[]{:S(2)}, u32[]{:S(2)}) async-start(bf16[8,48,2048]{2,1,0:T(8,128)(2,1)} %bitcast.63), calls=%async_computation | async-start | bytes 3145728 | tf_op jit(solution)/shard_map/all_to_all | solution.py:41
  32.5 20.6 %all-to-all-done = bf16[8,48,2048]{2,1,0:T(8,128)(2,1)S(1)} async-done(((bf16[8,48,2048]{2,1,0:T(8,128)(2,1)}), bf16[8,48,2048]{2,1,0:T(8,128)(2,1)S(1)}, u32[]{:S(2)}, u32[]{:S(2)}) %all-to-all-start) | async-done | bytes 1572896 | tf_op jit(solution)/shard_map/all_to_all | solution.py:41
  53.1 0.2 convert_reduce_fusion.1
  53.5 1.2 fusion.18
  55.0 24.0 %all_to_all.15 = bf16[8,48,2048]{2,1,0:T(8,128)(2,1)S(1)} all-to-all(bf16[8,48,2048]{2,1,0:T(8,128)(2,1)S(1)} %broadcast_in_dim.23), channel_id=1, replica_groups=mesh['sp'=64,'tp'=8] {'tp'}, dimensions={0} | all-to-all | bytes 3145728 | tf_op jit(solution)/shard_map/all_to_all | solution.py:53
  79.0 84.9 %all-gather.2.cloned.1.call-done = bf16[2048,2048]{1,0:T(8,128)(2,1)} async-done(((bf16[32,2048]{1,0:T(8,128)(2,1)}), bf16[2048,2048]{1,0:T(8,128)(2,1)}) %all-gather.2.cloned.1.call-update) | async-done | bytes 8388624 | tf_op jit(solution)/shard_map/all_gather | solution.py:13
  163.9 8.1 %fusion.4 = bf16[384,2048]{1,0:T(8,128)(2,1)} fusion(bf16[2048,2048]{1,0:T(8,128)(2,1)} %all-gather.2.cloned.1.call-done, bf16[384,2048]{1,0:T(8,128)(2,1)S(1)} %bitcast.64), kind=kOutput, calls=%fused_computation.6 | convolution fusion | flops 3223191552 | bytes 11534336 | tf_op jit(solution)/shard_map/dot_general | solution.py:147
  172.0 33.2 %all_to_all.16 = bf16[8,48,2048]{2,1,0:T(8,128)(2,1)S(1)} all-to-all(bf16[8,48,2048]{2,1,0:T(8,128)(2,1)} %bitcast.65), channel_id=1, replica_groups=mesh['sp'=64,'tp'=8] {'tp'}, dimensions={0} | all-to-all | bytes 3145728 | tf_op jit(solution)/shard_map/all_to_all | solution.py:41
  205.2 0.2 convert_reduce_fusion
  205.6 0.3 copy-done.4
  205.9 0.8 fusion.21
  (43 shorter events, 2.3 us)
Async XLA Ops:
  6.5 15.4 %copy-start = (bf16[256,2048]{1,0:T(8,128)(2,1)S(1)}, bf16[256,2048]{1,0:T(8,128)(2,1)}, u32[]{:S(2)}) copy-start(bf16[256,2048]{1,0:T(8,128)(2,1)} %param.18) | copy-start | bytes 3145732
  6.5 10.9 %copy-start.2 = (s32[24576]{0:T(1024)S(1)}, s32[24576]{0:T(1024)}, u32[]{:S(2)}) copy-start(s32[24576]{0:T(1024)} %param.16) | copy-start | bytes 294916
  6.5 157.3 %all-gather.2.cloned.1.call-start = ((), (), s32[]{:S(2)}) async-start(), calls=%async_computation.3 | async-start | bytes 8519680 | tf_op jit(solution)/shard_map/all_gather | solution.py:13
  10.1 8.9 %copy-start.1 = (bf16[384,128]{1,0:T(8,128)(2,1)S(1)}, bf16[384,128]{1,0:T(8,128)(2,1)}, u32[]{:S(2)}) copy-start(bf16[384,128]{1,0:T(8,128)(2,1)} %param.14) | copy-start | bytes 294916
  11.0 8.1 %collective-permute-start = (bf16[2,128,128]{2,1,0:T(8,128)(2,1)S(1)}, bf16[2,128,128]{2,1,0:T(8,128)(2,1)S(1)}, u32[]{:S(2)}, u32[]{:S(2)}) collective-permute-start(bf16[2,128,128]{2,1,0:T(8,128)(2,1)S(1)} %get-tuple-element.15), channel_id=1, source_target_pairs={{0,8},{8,16},{16,24},{24,32},{32,40},{40,48},{48,56},{56,64},{64,7... | collective-permute-start | bytes 196616 | tf_op jit(solution)/shard_map/ppermute | solution.py:28
  15.0 5.0 %collective-permute-start.1 = (bf16[2,128,128]{2,1,0:T(8,128)(2,1)S(1)}, bf16[2,128,128]{2,1,0:T(8,128)(2,1)S(1)}, u32[]{:S(2)}, u32[]{:S(2)}) collective-permute-start(bf16[2,128,128]{2,1,0:T(8,128)(2,1)S(1)} %get-tuple-element.16), channel_id=1, source_target_pairs={{8,0},{16,8},{24,16},{32,24},{40,32},{48,40},{56,48},{64,56},{72,6... | collective-permute-start | bytes 196616 | tf_op jit(solution)/shard_map/ppermute | solution.py:29
  20.1 0.7 copy-start.6
  23.7 29.4 %all-to-all-start = ((bf16[8,48,2048]{2,1,0:T(8,128)(2,1)}), bf16[8,48,2048]{2,1,0:T(8,128)(2,1)S(1)}, u32[]{:S(2)}, u32[]{:S(2)}) async-start(bf16[8,48,2048]{2,1,0:T(8,128)(2,1)} %bitcast.63), calls=%async_computation | async-start | bytes 3145728 | tf_op jit(solution)/shard_map/all_to_all | solution.py:41
  32.5 21.0 %copy-start.3 = (f32[2048]{0:T(1024)S(1)}, f32[2048]{0:T(1024)}, u32[]{:S(2)}) copy-start(f32[2048]{0:T(1024)} %param.19) | copy-start | bytes 24580
  32.5 22.2 %copy-start.5 = (f32[2048]{0:T(1024)S(1)}, f32[2048]{0:T(1024)}, u32[]{:S(2)}) copy-start(f32[2048]{0:T(1024)} %param.22) | copy-start | bytes 24580
  205.2 0.7 copy-start.4
Sparse Core Ops, SparseCore 0:
  10.3 153.5 all-gather.1
where the time goes:
time: 214 us
  waiting for transfers between devices  106 us (50%)
  blocking collectives  57.2 us (27%)
  starting transfers between devices  14.1 us (7%)
  between operations  13.6 us (6%)
  matrix products  10.8 us (5%)
  other arithmetic  8.61 us (4%)
  local copies, waits for them, and re-layouts  2.78 us (1%)
    all_gather x1, waiting for transfers between devices, turned_gather(): lax.all_gather(both, axis, axis=0, tiled=True)  84.9 us
    all_to_all x1, blocking collectives, summed_on_arrival(): lax.all_to_all(pieces, axis, split_axis=0, concat_axis=0, tiled=True)  33.2 us
    all_to_all x1, blocking collectives, copy_for_each(): lax.all_to_all(jnp.broadcast_to(shard[None], (devices, *shard.shape)), ax...  24 us
    all_to_all x1, waiting for transfers between devices, summed_on_arrival(): lax.all_to_all(pieces, axis, split_axis=0, concat_axis=0, tiled=True)  20.6 us
    all_to_all x1, starting transfers between devices, summed_on_arrival(): lax.all_to_all(pieces, axis, split_axis=0, concat_axis=0, tiled=True)  8.74 us
    dot_general x1, matrix products, body(): jnp.dot(hidden, down_whole, preferred_element_type=jnp.float32)  8.11 us
  transfers between devices with their start and end apart: 4, of which 3 were waited for; matrix products, arithmetic and copies ran while one was open for 5% of the time, Pallas kernels for 0%

commit v1 on v0

--- a/solution.py
+++ b/solution.py
@@ -10,7 +10,16 @@
 def turned_gather(arrays, axis, dims):
     turned = [jnp.moveaxis(a, dim, 0) for a, dim in zip(arrays, dims)]
     both = jnp.concatenate([t.reshape(len(t), -1) for t in turned], axis=1)
-    result, at, gathered = (lax.all_gather(both, axis, axis=0, tiled=True), 0, [])
+    result, at, gathered = (
+        jnp.concatenate(
+            lax.all_to_all(
+                jnp.stack(lax.axis_size(axis) * [both]), axis, split_axis=0, concat_axis=0
+            ),
+            axis=0,
+        ),
+        0,
+        [],
+    )
     for t, dim in zip(turned, dims):
         section = result[:, at : at + t[0].size].reshape(-1, *t.shape[1:])
         gathered.append(jnp.moveaxis(section, 0, dim))

time: 214 us -> 497 us (2.32)
  blocking collectives: 57.2 us -> 413 us
  waiting for transfers between devices: 106 us -> 41.2 us
  between operations: 13.6 us -> 0.26 us
    all_to_all x1, blocking collectives: 24 us -> 382 us  [turned_gather(): lax.all_to_all(jnp.stack(lax.axis_size(axis) * [both]), axis, split_axis=...]
    all_gather x1 -> x0, waiting for transfers between devices: 84.9 us -> none  [turned_gather(): lax.all_gather(both, axis, axis=0, tiled=True)]
    all_to_all x0 -> x1, waiting for transfers between devices: none -> 20.6 us  [copy_for_each(): lax.all_to_all(jnp.broadcast_to(shard[None], (devices, *shard.shape)), ax...]
  transfers between devices with their start and end apart: 4 -> 4, of which waited for: 3 -> 2; matrix products, arithmetic and copies ran while one was open for 5% -> 1% of each run, Pallas kernels for 0% -> 0%
where the time goes in v1:
time: 497 us
  blocking collectives  413 us (83%)
  waiting for transfers between devices  41.2 us (8%)
  starting transfers between devices  18.2 us (4%)
  matrix products  10.7 us (2%)
  other arithmetic  7.02 us (1%)
  local copies, waits for them, and re-layouts  6.6 us (1%)
    all_to_all x1, blocking collectives, turned_gather(): lax.all_to_all(jnp.stack(lax.axis_size(axis) * [both]), axis, split_axis=...  382 us
    all_to_all x1, blocking collectives, summed_on_arrival(): lax.all_to_all(pieces, axis, split_axis=0, concat_axis=0, tiled=True)  30.5 us
    all_to_all x1, waiting for transfers between devices, summed_on_arrival(): lax.all_to_all(pieces, axis, split_axis=0, concat_axis=0, tiled=True)  20.6 us
    all_to_all x1, waiting for transfers between devices, copy_for_each(): lax.all_to_all(jnp.broadcast_to(shard[None], (devices, *shard.shape)), ax...  20.6 us
  transfers between devices with their start and end apart: 4, of which 2 were waited for; matrix products, arithmetic and copies ran while one was open for 1% of the time, Pallas kernels for 0%

profile of v1, /device:TPU:1, one launch (start us, length us, event | category | flops | bytes accessed | tf_op | source)
XLA Modules:
  0.0 496.6 jit_solution(8760267173744208834)
XLA Ops:
  0.0 1.9 fusion.41
  1.9 0.9 pad_maximum_fusion.11
  2.8 4.0 collective-permute-start
  6.9 1.3 collective-permute-start.1
  8.2 0.4 multiply_cosine_fusion.1
  8.6 1.1 copy.26
  9.7 0.8 pad_dynamic-slice_fusion
  10.5 0.8 dynamic-slice_bitcast_fusion
  12.5 0.4 fusion.53
  13.2 0.3 fusion.14
  13.8 0.4 fusion.13
  14.4 1.7 convolution_convert_fusion
  16.1 8.3 %all-to-all-start = ((bf16[8,48,2048]{2,1,0:T(8,128)(2,1)}), bf16[8,48,2048]{2,1,0:T(8,128)(2,1)S(1)}, u32[]{:S(2)}, u32[]{:S(2)}) async-start(bf16[8,48,2048]{2,1,0:T(8,128)(2,1)} %bitcast.65), calls=%async_computation | async-start | bytes 3145728 | tf_op jit(solution)/shard_map/all_to_all | solution.py:50
  24.4 20.6 %all-to-all-done = bf16[8,48,2048]{2,1,0:T(8,128)(2,1)S(1)} async-done(((bf16[8,48,2048]{2,1,0:T(8,128)(2,1)}), bf16[8,48,2048]{2,1,0:T(8,128)(2,1)S(1)}, u32[]{:S(2)}, u32[]{:S(2)}) %all-to-all-start) | async-done | bytes 1572896 | tf_op jit(solution)/shard_map/all_to_all | solution.py:50
  45.4 1.2 fusion.18
  46.8 1.3 broadcast_in_dim.23
  48.1 4.6 all-to-all-start.1
  52.7 20.6 %all-to-all-done.1 = bf16[8,48,2048]{2,1,0:T(8,128)(2,1)S(1)} async-done(((bf16[8,48,2048]{2,1,0:T(8,128)(2,1)}), bf16[8,48,2048]{2,1,0:T(8,128)(2,1)S(1)}, u32[]{:S(2)}, u32[]{:S(2)}) %all-to-all-start.1) | async-done | bytes 1572896 | tf_op jit(solution)/shard_map/all_to_all | solution.py:62
  73.3 1.1 stack.8
  74.4 382.1 %all_to_all.20 = bf16[64,32,2048]{2,1,0:T(8,128)(2,1)} all-to-all(bf16[64,32,2048]{2,1,0:T(8,128)(2,1)S(1)} %stack.8), channel_id=1, replica_groups=mesh['sp'=64,'tp'=8] {'sp'}, dimensions={0} | all-to-all | bytes 16777216 | tf_op jit(solution)/shard_map/all_to_all | solution.py:15
  456.5 8.1 %fusion.4 = bf16[384,2048]{1,0:T(8,128)(2,1)} fusion(bf16[2048,2048]{1,0:T(8,128)(2,1)} %bitcast.64, bf16[384,2048]{1,0:T(8,128)(2,1)S(1)} %bitcast.66), kind=kOutput, calls=%fused_computation.6 | convolution fusion | flops 3223191552 | bytes 11534336 | tf_op jit(solution)/shard_map/dot_general | solution.py:156
  464.6 30.5 %all_to_all.21 = bf16[8,48,2048]{2,1,0:T(8,128)(2,1)S(1)} all-to-all(bf16[8,48,2048]{2,1,0:T(8,128)(2,1)} %bitcast.67), channel_id=1, replica_groups=mesh['sp'=64,'tp'=8] {'tp'}, dimensions={0} | all-to-all | bytes 3145728 | tf_op jit(solution)/shard_map/all_to_all | solution.py:50
  495.5 0.3 copy-done.5
  495.8 0.8 fusion.21
  (45 shorter events, 2.8 us)
Async XLA Ops:
  0.0 14.4 %copy-start = (bf16[256,2048]{1,0:T(8,128)(2,1)S(1)}, bf16[256,2048]{1,0:T(8,128)(2,1)}, u32[]{:S(2)}) copy-start(bf16[256,2048]{1,0:T(8,128)(2,1)} %param.18) | copy-start | bytes 3145732
  1.9 10.3 %copy-start.1 = (bf16[384,128]{1,0:T(8,128)(2,1)S(1)}, bf16[384,128]{1,0:T(8,128)(2,1)}, u32[]{:S(2)}) copy-start(bf16[384,128]{1,0:T(8,128)(2,1)} %param.14) | copy-start | bytes 294916
  2.8 9.5 %collective-permute-start = (bf16[2,128,128]{2,1,0:T(8,128)(2,1)S(1)}, bf16[2,128,128]{2,1,0:T(8,128)(2,1)S(1)}, u32[]{:S(2)}, u32[]{:S(2)}) collective-permute-start(bf16[2,128,128]{2,1,0:T(8,128)(2,1)S(1)} %get-tuple-element.15), channel_id=1, source_target_pairs={{0,8},{8,16},{16,24},{24,32},{32,40},{40,48},{48,56},{56,64},{64,7... | collective-permute-start | bytes 196616 | tf_op jit(solution)/shard_map/ppermute | solution.py:37
  6.9 5.4 %collective-permute-start.1 = (bf16[2,128,128]{2,1,0:T(8,128)(2,1)S(1)}, bf16[2,128,128]{2,1,0:T(8,128)(2,1)S(1)}, u32[]{:S(2)}, u32[]{:S(2)}) collective-permute-start(bf16[2,128,128]{2,1,0:T(8,128)(2,1)S(1)} %get-tuple-element.16), channel_id=1, source_target_pairs={{8,0},{16,8},{24,16},{32,24},{40,32},{48,40},{56,48},{64,56},{72,6... | collective-permute-start | bytes 196616 | tf_op jit(solution)/shard_map/ppermute | solution.py:38
  12.4 0.7 copy-start.7
  16.1 28.9 %all-to-all-start = ((bf16[8,48,2048]{2,1,0:T(8,128)(2,1)}), bf16[8,48,2048]{2,1,0:T(8,128)(2,1)S(1)}, u32[]{:S(2)}, u32[]{:S(2)}) async-start(bf16[8,48,2048]{2,1,0:T(8,128)(2,1)} %bitcast.65), calls=%async_computation | async-start | bytes 3145728 | tf_op jit(solution)/shard_map/all_to_all | solution.py:50
  24.4 21.0 %copy-start.4 = (f32[2048]{0:T(1024)S(1)}, f32[2048]{0:T(1024)}, u32[]{:S(2)}) copy-start(f32[2048]{0:T(1024)} %param.19) | copy-start | bytes 24580
  24.4 22.2 %copy-start.6 = (f32[2048]{0:T(1024)S(1)}, f32[2048]{0:T(1024)}, u32[]{:S(2)}) copy-start(f32[2048]{0:T(1024)} %param.22) | copy-start | bytes 24580
  48.1 4.6 copy-start.2
  48.1 4.6 copy-start.3
  48.1 25.2 %all-to-all-start.1 = ((bf16[8,48,2048]{2,1,0:T(8,128)(2,1)}), bf16[8,48,2048]{2,1,0:T(8,128)(2,1)S(1)}, u32[]{:S(2)}, u32[]{:S(2)}) async-start(bf16[8,48,2048]{2,1,0:T(8,128)(2,1)} %broadcast_in_dim.23), calls=%async_computation.1 | async-start | bytes 3145728 | tf_op jit(solution)/shard_map/all_to_all | solution.py:62
  495.1 0.7 copy-start.5
